TPU v7x, 32 devices: a whole 2x2x4 slice. The times are simulated.
32 devices in a mesh: ep: 4 (over y, x), tp: 8 (over z, core).
Axes of the slice: x: 2, y: 2, z: 4, core: 2. Of those that a mesh axis runs over, the one named last changes fastest.
Arguments:
- tokens: bfloat16 [64, 2048], P('ep'), may hold values from -6 to 6
- routes: int32 [64, 4], P('ep'), may hold values from 0 to 7, all different within a row; in each aligned block of 16 rows (0 to 15, 16 to 31, ...) at most 16 rows name the same one
- route_weight: float32 [64, 4], P('ep'), may hold values from 0.2 to 1
- mixer_gain: float32 [2048], replicated, may hold values from 0.1 to 1.9
- gate_weight: bfloat16 [2048, 4096], P(None, 'tp'), may hold values from -0.125 to 0.125
- input_weight: bfloat16 [2048, 4096], P(None, 'tp'), may hold values from -0.125 to 0.125
- step_weight: bfloat16 [2048, 64], P(None, 'tp'), may hold values from -0.125 to 0.125
- write_weight: bfloat16 [2048, 512], P('tp'), may hold values from -0.125 to 0.125
- read_weight: bfloat16 [2048, 512], P('tp'), may hold values from -0.125 to 0.125
- step_bias: float32 [64], P('tp'), may hold values from -3 to 0.5
- decay_log: float32 [64], P('tp'), may hold values from -2 to 0.5
- decay_jolt: float32 [64, 64], P('ep', 'tp'), may hold values from -1 to 0
- filter_taps: bfloat16 [4, 4096], P(None, 'tp'), may hold values from -3 to 3
- filter_state: bfloat16 [64, 3, 4096], P('ep', None, 'tp'), may hold values from -6 to 6
- scan_state: float32 [64, 64, 64, 128], P('ep', 'tp'), may hold values from -2 to 2
- skip_gain: float32 [64], P('tp'), may hold values from 0.5 to 2
- head_gain: float32 [4096], P('tp'), may hold values from 0.1 to 1.9
- output_weight: bfloat16 [4096, 2048], P('tp'), may hold values from -0.09375 to 0.09375
- channel_gain: float32 [2048], replicated, may hold values from 0.1 to 1.9
- expert_gate: bfloat16 [8, 2048, 2048], P('ep', None, 'tp'), may hold values from -0.125 to 0.125
- expert_up: bfloat16 [8, 2048, 2048], P('ep', None, 'tp'), may hold values from -0.125 to 0.125
- expert_down: bfloat16 [8, 2048, 2048], P('ep', 'tp'), may hold values from -0.125 to 0.125
- shared_gate: bfloat16 [2048, 2048], P(None, 'tp'), may hold values from -0.125 to 0.125
- shared_up: bfloat16 [2048, 2048], P(None, 'tp'), may hold values from -0.125 to 0.125
- shared_down: bfloat16 [2048, 2048], P('tp'), may hold values from -0.125 to 0.125
Outputs:
- layer_out: bfloat16 [64, 2048], P('ep', 'tp')
- new_state: float32 [64, 64, 64, 128], P('ep', 'tp')
- new_filter: bfloat16 [64, 3, 4096], P('ep', None, 'tp')
Inputs may be any that keep to these rules, and one draw needn't show every extreme that they name: `routes`: each row names 4 different experts. In each aligned block of 16 rows (the rows of one index of ep) no expert is named by more than 16 rows, a bound that some block reaches.
All inputs are finite; a program needn't handle non-finite values.
Results may differ from a plain program's by a relative error of at most 0.025.
Values may be sent and summed in bfloat16 or wider, within the bound.
A program may use at most 64 MiB of HBM per device.

v0:
```python
import functools

import jax
import jax.numpy as jnp
from jax import lax
from jax.experimental import pallas as pl
from jax.experimental.pallas import tpu as pltpu
from jax.sharding import PartitionSpec as P

HEADS = 64
HEAD_DIM = 64
GROUPS = 4
STATE = 128

EPS = 1e-06
F32 = jnp.float32
BF16 = jnp.bfloat16
MESH = pl.DeviceIdType.MESH
VMEM_LIMIT = 56 * 1024 * 1024


def dot(a, b):
    return jnp.dot(a, b, preferred_element_type=F32)


def dot_nt(a, b):
    return lax.dot_general(a, b, (((1,), (1,)), ((), ())), preferred_element_type=F32)


def split(v):
    high = v.astype(BF16)
    return high, (v - high.astype(F32)).astype(BF16)


def softplus(v):
    return jnp.maximum(v, 0.0) + jnp.log1p(jnp.exp(-jnp.abs(v)))


def project_kernel(
    n_tp,
    heads_here,
    tokens_ref,
    gain_ref,
    step_ref,
    gate_hbm,
    input_hbm,
    write_hbm,
    read_hbm,
    vec_ref,
    gate_ref,
    input_ref,
    raw_ref,
    gate_buf,
    input_buf,
    write_buf,
    read_buf,
    normed_buf,
    out_buf,
    in_buf,
    load_sem,
    send_sem,
    recv_sem,
):
    ep = lax.axis_index("ep")
    tp = lax.axis_index("tp")
    loads = [
        pltpu.make_async_copy(src, dst, load_sem.at[i])
        for i, (src, dst) in enumerate(
            (
                (write_hbm, write_buf),
                (read_hbm, read_buf),
                (input_hbm, input_buf),
                (gate_hbm, gate_buf),
            )
        )
    ]
    for load in loads:
        load.start()
    barrier = pltpu.get_barrier_semaphore()

    def greet(k, carry):
        pl.semaphore_signal(
            barrier, inc=1, device_id=(ep, lax.rem(tp + k, n_tp)), device_id_type=MESH
        )
        return carry

    lax.fori_loop(1, n_tp, greet, 0)
    tokens = tokens_ref[...].astype(F32)
    scale = lax.rsqrt(jnp.mean(tokens * tokens, axis=-1, keepdims=True) + EPS)
    normed_buf[...] = (tokens * scale * gain_ref[...]).astype(BF16)
    features = write_buf.shape[0]
    own = normed_buf[:, pl.ds(pl.multiple_of(tp * features, features), features)]
    loads[0].wait()
    loads[1].wait()
    write_part = dot(own, write_buf[...]).astype(BF16)
    read_part = dot(own, read_buf[...]).astype(BF16)
    for g in range(GROUPS):
        out_buf[g, :, :STATE] = write_part[:, g * STATE : (g + 1) * STATE]
        out_buf[g, :, STATE:] = read_part[:, g * STATE : (g + 1) * STATE]
    per_group = HEADS // GROUPS
    pl.semaphore_wait(barrier, n_tp - 1)

    def copy_to(k):
        peer = lax.rem(tp + k, n_tp)
        return pltpu.make_async_remote_copy(
            src_ref=out_buf.at[(peer * heads_here) // per_group],
            dst_ref=in_buf.at[tp],
            send_sem=send_sem.at[peer],
            recv_sem=recv_sem.at[tp],
            device_id=(ep, peer),
            device_id_type=MESH,
        )

    def copy_from(k):
        peer = lax.rem(tp + k, n_tp)
        return pltpu.make_async_remote_copy(
            src_ref=out_buf.at[0],
            dst_ref=in_buf.at[peer],
            send_sem=send_sem.at[peer],
            recv_sem=recv_sem.at[peer],
            device_id=(ep, peer),
            device_id_type=MESH,
        )

    def send(k, carry):
        copy_to(k).start()
        return carry

    lax.fori_loop(1, n_tp, send, 0)
    in_buf[tp] = out_buf[(tp * heads_here) // per_group]
    normed = normed_buf[...]
    raw_ref[...] = dot_nt(step_ref[...], normed)
    loads[2].wait()
    input_ref[...] = dot(normed, input_buf[...]).astype(BF16)
    loads[3].wait()
    gate_ref[...] = dot(normed, gate_buf[...]).astype(BF16)

    def receive(k, carry):
        copy_from(k).wait_recv()
        return carry

    lax.fori_loop(1, n_tp, receive, 0)
    vec_ref[...] = jax.nn.silu(jnp.sum(in_buf[...].astype(F32), axis=0))

    def sent(k, carry):
        copy_to(k).wait_send()
        return carry

    lax.fori_loop(1, n_tp, sent, 0)


def state_kernel(
    bias_ref,
    rate_ref,
    skip_ref,
    vec_ref,
    gate_ref,
    input_ref,
    raw_ref,
    jolt_ref,
    taps_ref,
    filter_ref,
    gain_ref,
    state_hbm,
    weight_hbm,
    part_ref,
    new_hbm,
    new_filter_ref,
    state_buf,
    new_buf,
    weight_buf,
    decay_buf,
    x_buf,
    read_buf,
    load_sem,
    store_sem,
    weight_sem,
):
    rows, width, _ = state_buf.shape
    heads = jolt_ref.shape[0]
    for s in range(rows):
        pltpu.make_async_copy(state_hbm.at[s], state_buf.at[s], load_sem.at[s]).start()
    weight_load = pltpu.make_async_copy(weight_hbm, weight_buf, weight_sem)
    weight_load.start()
    taps = taps_ref[...].astype(F32)
    last = filter_ref.shape[0]
    inputs = input_ref[...]
    total = inputs.astype(F32) * taps[last : last + 1]
    for i in range(last):
        total = total + filter_ref[i].astype(F32) * taps[i : i + 1]
        new_filter_ref[i] = filter_ref[i + 1] if i + 1 < last else inputs
    filtered = jax.nn.silu(total)
    pad = jnp.zeros((128 - rows, width), F32)
    filtered_t = jnp.transpose(jnp.concatenate([filtered, pad], axis=0))[:, :rows]
    head_ids = lax.broadcasted_iota(jnp.int32, (heads, rows), 0)
    bias = jnp.zeros((heads, rows), F32)
    rate = jnp.zeros((heads, rows), F32)
    for h in range(heads):
        bias = jnp.where(head_ids == h, bias_ref[h], bias)
        rate = jnp.where(head_ids == h, rate_ref[h], rate)
    step = softplus(raw_ref[...] + bias)
    decay = jnp.exp(jolt_ref[...] - jnp.exp(rate) * step)

    def expand(v):
        return jnp.concatenate(
            [jnp.broadcast_to(v[h : h + 1], (HEAD_DIM, rows)) for h in range(heads)], axis=0
        )

    decay_buf[...] = expand(decay)
    x_buf[...] = expand(step) * filtered_t
    for s in range(rows):
        pltpu.make_async_copy(state_hbm.at[s], state_buf.at[s], load_sem.at[s]).wait()
        write = vec_ref[s : s + 1, :STATE]
        new = decay_buf[:, s : s + 1] * state_buf[s] + x_buf[:, s : s + 1] * write
        new_buf[s] = new
        pltpu.make_async_copy(new_buf.at[s], new_hbm.at[s], store_sem.at[s]).start()
        read_high, read_low = split(vec_ref[s : s + 1, STATE:])
        high, low = split(new)
        read_buf[s : s + 1, :] = (
            dot_nt(read_high, high) + dot_nt(read_low, high) + dot_nt(read_high, low)
        )
    lane_head = lax.broadcasted_iota(jnp.int32, (1, width), 1) // HEAD_DIM
    skip = jnp.zeros((1, width), F32)
    for h in range(heads):
        skip = jnp.where(lane_head == h, skip_ref[h], skip)
    value = (read_buf[...] + skip * filtered) * jax.nn.silu(gate_ref[...].astype(F32))
    same = (
        lax.broadcasted_iota(jnp.int32, (width, width), 0) // HEAD_DIM
        == lax.broadcasted_iota(jnp.int32, (width, width), 1) // HEAD_DIM
    )
    block = jnp.where(same, 1.0, 0.0).astype(BF16)
    high, low = split(value * value)
    mean_square = (dot(high, block) + dot(low, block)) * (1.0 / HEAD_DIM)
    gated = (value * lax.rsqrt(mean_square + EPS) * gain_ref[...]).astype(BF16)
    weight_load.wait()
    columns = part_ref.shape[2]
    for t in range(part_ref.shape[0]):
        part_ref[t] = dot(gated, weight_buf[:, t * columns : (t + 1) * columns]).astype(BF16)
    for s in range(rows):
        pltpu.make_async_copy(new_buf.at[s], new_hbm.at[s], store_sem.at[s]).wait()


def expert_kernel(
    n_ep,
    n_tp,
    part_ref,
    tokens_ref,
    routes_ref,
    route_weight_ref,
    gain_ref,
    gate_hbm,
    up_hbm,
    down_hbm,
    sgate_hbm,
    sup_hbm,
    sdown_hbm,
    out_ref,
    gate_buf,
    up_buf,
    down_buf,
    sgate_buf,
    sup_buf,
    sdown_buf,
    mix_buf,
    resid_buf,
    share_buf,
    normed_buf,
    total_buf,
    shared_buf,
    term_buf,
    back_buf,
    load_sem,
    mix_send,
    mix_recv,
    share_send,
    share_recv,
    resid_send,
    resid_recv,
    back_send,
    back_recv,
):
    ep = lax.axis_index("ep")
    tp = lax.axis_index("tp")
    me = ep * n_tp + tp
    n_all = n_ep * n_tp
    rows, columns = out_ref.shape
    loads = [
        pltpu.make_async_copy(src, dst, load_sem.at[i])
        for i, (src, dst) in enumerate(
            (
                (sgate_hbm, sgate_buf),
                (sup_hbm, sup_buf),
                (sdown_hbm, sdown_buf),
                (gate_hbm, gate_buf),
                (up_hbm, up_buf),
                (down_hbm, down_buf),
            )
        )
    ]
    barrier = pltpu.get_barrier_semaphore()

    def place(k):
        other = lax.rem(me + k, n_all)
        return other // n_tp, lax.rem(other, n_tp)

    def loop(low, high, act):
        def body(k, carry):
            act(k)
            return carry

        lax.fori_loop(low, high, body, 0)

    loop(
        1,
        n_all,
        lambda k: pl.semaphore_signal(barrier, inc=1, device_id=place(k), device_id_type=MESH),
    )
    for load in loads:
        load.start()

    lanes = share_buf.shape[2]
    ids = lax.broadcasted_iota(jnp.int32, (lanes, rows), 0)
    share = jnp.zeros((lanes, rows), F32)
    for k in range(routes_ref.shape[0]):
        share = share + jnp.where(
            routes_ref[k : k + 1, :] == ids, route_weight_ref[k : k + 1, :], 0.0
        )
    pad = jnp.zeros((lanes, 128 - rows), F32)
    share_buf[ep] = jnp.transpose(jnp.concatenate([share, pad], axis=1))[:rows]

    def mix_copy(k, slot):
        peer = lax.rem(tp + k, n_tp)
        return pltpu.make_async_remote_copy(
            src_ref=part_ref.at[peer],
            dst_ref=mix_buf.at[tp if slot is None else peer],
            send_sem=mix_send.at[peer],
            recv_sem=mix_recv.at[tp if slot is None else peer],
            device_id=(ep, peer),
            device_id_type=MESH,
        )

    def share_copy(k, slot):
        peer = lax.rem(ep + k, n_ep)
        mine = ep if slot is None else peer
        return pltpu.make_async_remote_copy(
            src_ref=share_buf.at[mine],
            dst_ref=share_buf.at[mine],
            send_sem=share_send.at[peer],
            recv_sem=share_recv.at[mine],
            device_id=(peer, tp),
            device_id_type=MESH,
        )

    def resid_copy(e, t, slot):
        at_e, at_t = (ep, tp) if slot is None else (e, t)
        return pltpu.make_async_remote_copy(
            src_ref=resid_buf.at[at_e, at_t],
            dst_ref=resid_buf.at[at_e, at_t],
            send_sem=resid_send.at[e * n_tp + t],
            recv_sem=resid_recv.at[at_e * n_tp + at_t],
            device_id=(e, t),
            device_id_type=MESH,
        )

    def back_copy(e, t, slot):
        at_e, at_t = (ep, tp) if slot is None else (e, t)
        return pltpu.make_async_remote_copy(
            src_ref=term_buf.at[t, e],
            dst_ref=back_buf.at[at_e * n_tp + at_t],
            send_sem=back_send.at[e * n_tp + t],
            recv_sem=back_recv.at[at_e * n_tp + at_t],
            device_id=(e, t),
            device_id_type=MESH,
        )

    pl.semaphore_wait(barrier, n_all - 1)
    loop(1, n_tp, lambda k: mix_copy(k, None).start())
    loop(1, n_ep, lambda k: share_copy(k, None).start())
    mix_buf[tp] = part_ref[tp]
    own_tokens = tokens_ref[:, pl.ds(pl.multiple_of(tp * columns, columns), columns)]
    loop(1, n_tp, lambda k: mix_copy(k, 1).wait_recv())
    mixed = jnp.sum(mix_buf[...].astype(F32), axis=0).astype(BF16)
    resid_own = (own_tokens.astype(F32) + mixed.astype(F32)).astype(BF16)
    resid_buf[ep, tp] = resid_own
    def own_group(act):
        loop(1, n_tp, lambda k: act(ep, lax.rem(tp + k, n_tp)))

    def other_groups(act):
        def body(k):
            act(lax.rem(ep + 1 + k // n_tp, n_ep), lax.rem(tp + lax.rem(k, n_tp), n_tp))

        loop(0, (n_ep - 1) * n_tp, body)

    own_group(lambda e, t: resid_copy(e, t, None).start())
    other_groups(lambda e, t: resid_copy(e, t, None).start())

    def normalise(e):
        square = jnp.zeros((rows, columns), F32)
        for t in range(n_tp):
            value = resid_buf[e, t].astype(F32)
            square = square + value * value
        mean_square = jnp.sum(square, axis=-1, keepdims=True) * (1.0 / (n_tp * columns))
        scale = lax.rsqrt(mean_square + EPS)
        for t in range(n_tp):
            at = slice(t * columns, (t + 1) * columns)
            value = resid_buf[e, t].astype(F32) * scale * gain_ref[:, at]
            normed_buf[pl.ds(pl.multiple_of(e * rows, rows), rows), at] = value.astype(BF16)

    own_group(lambda e, t: resid_copy(e, t, 1).wait_recv())
    normalise(ep)
    normed_own = normed_buf[pl.ds(pl.multiple_of(ep * rows, rows), rows), :]
    loads[0].wait()
    loads[1].wait()
    shared_hidden = (
        jax.nn.silu(dot(normed_own, sgate_buf[...])) * dot(normed_own, sup_buf[...])
    ).astype(BF16)
    loads[2].wait()
    for t in range(n_tp):
        at = slice(t * columns, (t + 1) * columns)
        shared_buf[t] = dot(shared_hidden, sdown_buf[:, at])
    other_groups(lambda e, t: resid_copy(e, t, 1).wait_recv())
    loop(1, n_ep, lambda k: normalise(lax.rem(ep + k, n_ep)))
    loads[3].wait()
    loads[4].wait()
    hidden = []
    for j in range(gate_buf.shape[0]):
        normed = normed_buf[...]
        hidden.append(
            (jax.nn.silu(dot(normed, gate_buf[j])) * dot(normed, up_buf[j])).astype(BF16)
        )
    loop(1, n_ep, lambda k: share_copy(k, 1).wait_recv())
    shares = share_buf[...].reshape(n_ep * rows, lanes)
    all_lanes = lax.broadcasted_iota(jnp.int32, shares.shape, 1)
    local = gate_buf.shape[0]
    scales = [
        jnp.sum(jnp.where(all_lanes == ep * local + j, shares, 0.0), axis=1, keepdims=True)
        for j in range(local)
    ]
    loads[5].wait()
    for t in range(n_tp):
        at = slice(t * columns, (t + 1) * columns)
        term = scales[0] * dot(hidden[0], down_buf[0, :, at])
        for j in range(1, local):
            term = term + scales[j] * dot(hidden[j], down_buf[j, :, at])
        total_buf[t] = term.reshape(n_ep, rows, columns)
        total_buf[t, ep] = total_buf[t, ep] + shared_buf[t]
        term_buf[t] = total_buf[t].astype(BF16)

        def give(e):
            @pl.when(e * n_tp + t != me)
            def _():
                back_copy(e, t, None).start()

        loop(0, n_ep, give)
    back_buf[me] = term_buf[tp, ep]

    def others(act):
        def body(k):
            e, t = place(k)
            act(e, t)

        loop(1, n_all, body)

    others(lambda e, t: back_copy(e, t, 1).wait_recv())
    out_ref[...] = (
        resid_buf[ep, tp].astype(F32) + jnp.sum(back_buf[...].astype(F32), axis=0)
    ).astype(BF16)
    loop(1, n_tp, lambda k: mix_copy(k, None).wait_send())
    loop(1, n_ep, lambda k: share_copy(k, None).wait_send())
    own_group(lambda e, t: resid_copy(e, t, None).wait_send())
    other_groups(lambda e, t: resid_copy(e, t, None).wait_send())
    others(lambda e, t: back_copy(e, t, None).wait_send())


def on_device(
    tokens,
    routes,
    route_weight,
    mixer_gain,
    gate_weight,
    input_weight,
    step_weight,
    write_weight,
    read_weight,
    step_bias,
    decay_log,
    decay_jolt,
    filter_taps,
    filter_state,
    scan_state,
    skip_gain,
    head_gain,
    output_weight,
    channel_gain,
    expert_gate,
    expert_up,
    expert_down,
    shared_gate,
    shared_up,
    shared_down,
):
    rows, model = tokens.shape
    n_tp = lax.axis_size("tp")
    n_ep = lax.axis_size("ep")
    n_all = n_tp * n_ep
    columns = model // n_tp
    heads_here = step_bias.shape[0]
    width = gate_weight.shape[1]
    vmem = pl.BlockSpec(memory_space=pltpu.VMEM)
    smem = pl.BlockSpec(memory_space=pltpu.SMEM)
    hbm = pl.BlockSpec(memory_space=pl.ANY)
    dma = pltpu.SemaphoreType.DMA
    shape = jax.ShapeDtypeStruct

    vecs, gate_rows, input_rows, step_raw = pl.pallas_call(
        functools.partial(project_kernel, n_tp, heads_here),
        out_shape=(
            shape((rows, 2 * STATE), F32),
            shape((rows, width), BF16),
            shape((rows, width), BF16),
            shape((heads_here, rows), F32),
        ),
        in_specs=[vmem] * 3 + [hbm] * 4,
        out_specs=(vmem,) * 4,
        scratch_shapes=[
            pltpu.VMEM(gate_weight.shape, BF16),
            pltpu.VMEM(input_weight.shape, BF16),
            pltpu.VMEM(write_weight.shape, BF16),
            pltpu.VMEM(read_weight.shape, BF16),
            pltpu.VMEM((rows, model), BF16),
            pltpu.VMEM((GROUPS, rows, 2 * STATE), BF16),
            pltpu.VMEM((n_tp, rows, 2 * STATE), BF16),
            dma((4,)),
            dma((n_tp,)),
            dma((n_tp,)),
        ],
        compiler_params=pltpu.CompilerParams(
            collective_id=0, has_side_effects=True, vmem_limit_bytes=VMEM_LIMIT
        ),
        name="project",
    )(
        tokens,
        mixer_gain.reshape(1, model),
        step_weight.T,
        gate_weight,
        input_weight,
        write_weight,
        read_weight,
    )

    taps = filter_state.shape[1]
    part, new_state, new_filter = pl.pallas_call(
        state_kernel,
        out_shape=(
            shape((n_tp, rows, columns), BF16),
            shape((rows, width, STATE), F32),
            shape((taps, rows, width), BF16),
        ),
        in_specs=[smem] * 3 + [vmem] * 8 + [hbm] * 2,
        out_specs=(vmem, hbm, vmem),
        scratch_shapes=[
            pltpu.VMEM((rows, width, STATE), F32),
            pltpu.VMEM((rows, width, STATE), F32),
            pltpu.VMEM(output_weight.shape, BF16),
            pltpu.VMEM((width, rows), F32),
            pltpu.VMEM((width, rows), F32),
            pltpu.VMEM((rows, width), F32),
            dma((rows,)),
            dma((rows,)),
            dma,
        ],
        compiler_params=pltpu.CompilerParams(vmem_limit_bytes=VMEM_LIMIT),
        name="state",
    )(
        step_bias,
        decay_log,
        skip_gain,
        vecs,
        gate_rows,
        input_rows,
        step_raw,
        decay_jolt.T,
        filter_taps,
        jnp.transpose(filter_state, (1, 0, 2)),
        head_gain.reshape(1, width),
        scan_state.reshape(rows, width, STATE),
        output_weight,
    )

    experts = expert_gate.shape[0] * n_ep
    lanes = -(-experts // 128) * 128
    layer_out = pl.pallas_call(
        functools.partial(expert_kernel, n_ep, n_tp),
        out_shape=shape((rows, columns), BF16),
        in_specs=[vmem] * 5 + [hbm] * 6,
        out_specs=vmem,
        scratch_shapes=[
            pltpu.VMEM(expert_gate.shape, BF16),
            pltpu.VMEM(expert_up.shape, BF16),
            pltpu.VMEM(expert_down.shape, BF16),
            pltpu.VMEM(shared_gate.shape, BF16),
            pltpu.VMEM(shared_up.shape, BF16),
            pltpu.VMEM(shared_down.shape, BF16),
            pltpu.VMEM((n_tp, rows, columns), BF16),
            pltpu.VMEM((n_ep, n_tp, rows, columns), BF16),
            pltpu.VMEM((n_ep, rows, lanes), F32),
            pltpu.VMEM((n_ep * rows, model), BF16),
            pltpu.VMEM((n_tp, n_ep, rows, columns), F32),
            pltpu.VMEM((n_tp, rows, columns), F32),
            pltpu.VMEM((n_tp, n_ep, rows, columns), BF16),
            pltpu.VMEM((n_all, rows, columns), BF16),
            dma((6,)),
            dma((n_tp,)),
            dma((n_tp,)),
            dma((n_ep,)),
            dma((n_ep,)),
            dma((n_all,)),
            dma((n_all,)),
            dma((n_all,)),
            dma((n_all,)),
        ],
        compiler_params=pltpu.CompilerParams(
            collective_id=1, has_side_effects=True, vmem_limit_bytes=VMEM_LIMIT
        ),
        name="experts",
    )(
        part,
        tokens,
        routes.T,
        route_weight.T,
        channel_gain.reshape(1, model),
        expert_gate,
        expert_up,
        expert_down,
        shared_gate,
        shared_up,
        shared_down,
    )
    return (
        layer_out,
        new_state.reshape(scan_state.shape),
        jnp.transpose(new_filter, (1, 0, 2)),
    )


def solution(mesh):
    in_specs = (
        P("ep", None),
        P("ep", None),
        P("ep", None),
        P(),
        P(None, "tp"),
        P(None, "tp"),
        P(None, "tp"),
        P("tp", None),
        P("tp", None),
        P("tp"),
        P("tp"),
        P("ep", "tp"),
        P(None, "tp"),
        P("ep", None, "tp"),
        P("ep", "tp", None, None),
        P("tp"),
        P("tp"),
        P("tp", None),
        P(),
        P("ep", None, "tp"),
        P("ep", None, "tp"),
        P("ep", "tp", None),
        P(None, "tp"),
        P(None, "tp"),
        P("tp", None),
    )
    out_specs = (P("ep", "tp"), P("ep", "tp", None, None), P("ep", None, "tp"))
    return jax.shard_map(
        on_device, mesh=mesh, in_specs=in_specs, out_specs=out_specs, check_vma=False
    )
```

profile of v0, /device:TPU:25, one launch (start us, length us, event | category | flops | bytes accessed | tf_op | source)
XLA Modules:
  0.0 50.2 jit_solution(1757963905947748010)
XLA Ops:
  0.6 7.8 %project.1 = (f32[16,256]{1,0:T(8,128)}, bf16[16,512]{1,0:T(8,128)(2,1)}, bf16[16,512]{1,0:T(8,128)(2,1)}, f32[8,16]{1,0:T(8,128)}) custom-call(bf16[16,2048]{1,0:T(8,128)(2,1)} %tokens_ref.3, f32[1,2048]{1,0:T(1,128)} %bitcast.14, bf16[8,2048]{1,0:T(8,128)(2,1)} %bitcast.13, bf16[2048,512]{1,0:T(8,128)(2,1)} %gate_hbm.2, bf16[2048,512]{1,0:T(8,128)(2,1)} %input_hbm.1, ...), custom_call_target="tpu_custom_call" | custom-call | tf_op jit(solution)/shard_map/project/pallas_call | solution.py:515
  8.5 9.7 %state.1 = (bf16[8,16,256]{2,1,0:T(8,128)(2,1)}, f32[16,512,128]{2,1,0:T(8,128)}, bf16[3,16,512]{2,1,0:T(8,128)(2,1)}) custom-call(f32[8]{0:T(128)} %bias_ref.1, f32[8]{0:T(128)} %rate_ref.1, f32[8]{0:T(128)} %skip_ref.1, f32[16,256]{1,0:T(8,128)} %get-tuple-element.10.vec_ref, bf16[16,512]{1,0:T(8,128)(2,1)} %get-tuple-element.11.gate_ref, ...), custom_call_target="tpu_custom_call" | custom-call | tf_op jit(solution)/shard_map/state/pallas_call | solution.py:552
  18.2 30.6 %experts.1 = bf16[16,256]{1,0:T(8,128)(2,1)} custom-call(bf16[8,16,256]{2,1,0:T(8,128)(2,1)} %get-tuple-element.14.part_ref, bf16[16,2048]{1,0:T(8,128)(2,1)} %tokens_ref.3, s32[4,16]{1,0:T(4,128)} %bitcast.18, f32[4,16]{1,0:T(4,128)} %bitcast.19, f32[1,2048]{1,0:T(1,128)} %bitcast.15, bf16[2,2048,256]{2,1,0:T(8,128)(2,1)} %gate_hbm.3, ...), custom_call_target="tpu_custom_call" | custom-call | tf_op jit(solution)/shard_map/experts/pallas_call | solution.py:592
  48.9 1.3 %copy.29 = bf16[16,256]{1,0:T(8,128)(2,1)} copy(bf16[16,256]{1,0:T(8,128)(2,1)} %experts.1) | data formatting | bytes 16384
where the time goes:
time: 50.5 us; the launch traced here: 50.2 us
  Pallas kernels  48.2 us (95%)
  local copies, waits for them, and re-layouts  1.3 us (3%)
  between operations  0.66 us (1%)
    pallas_call x1, Pallas kernels, on_device(): pl.pallas_call(functools.partial(expert_kernel, n_ep, n_tp), out_shape=sh...  30.6 us
    pallas_call x1, Pallas kernels, on_device(): pl.pallas_call(state_kernel, out_shape=(shape((n_tp, rows, columns), BF16...  9.74 us
    pallas_call x1, Pallas kernels, on_device(): pl.pallas_call(functools.partial(project_kernel, n_tp, heads_here), out_s...  7.85 us
    unnamed x1, local copies, waits for them, and re-layouts  1.3 us

commit v1 on v0

v1 whole, which is shorter than its diff:
```python
import functools

import jax
import jax.numpy as jnp
from jax import lax
from jax.experimental import pallas as pl
from jax.experimental.pallas import tpu as pltpu
from jax.sharding import PartitionSpec as P

HEADS = 64
HEAD_DIM = 64
GROUPS = 4
STATE = 128

EPS = 1e-06
F32 = jnp.float32
BF16 = jnp.bfloat16
MESH = pl.DeviceIdType.MESH
VMEM_LIMIT = 67043328
SPARE = 64 * 1024
LANES = 128


def dot(a, b):
    return jnp.dot(a, b, preferred_element_type=F32)


def dot_nt(a, b):
    return lax.dot_general(a, b, (((1,), (1,)), ((), ())), preferred_element_type=F32)


def split(v):
    high = v.astype(BF16)
    return high, (v - high.astype(F32)).astype(BF16)


def softplus(v):
    return jnp.maximum(v, 0.0) + jnp.log1p(jnp.exp(-jnp.abs(v)))


def far_first(n):
    return sorted(range(n), key=lambda k: -min(k, n - k))


def loop(low, high, act):
    if high - low <= 32:
        for k in range(low, high):
            act(k)
        return

    def body(k, carry):
        act(k)
        return carry

    lax.fori_loop(low, high, body, 0)


def layer_kernel(
    n_ep,
    n_tp,
    tokens_hbm,
    routes_hbm,
    share_hbm,
    mgain_hbm,
    gate_hbm,
    input_hbm,
    step_hbm,
    write_hbm,
    read_hbm,
    bias_hbm,
    rate_hbm,
    jolt_hbm,
    taps_hbm,
    filter_hbm,
    state_hbm,
    skip_hbm,
    hgain_hbm,
    outw_hbm,
    cgain_hbm,
    egate_hbm,
    eup_hbm,
    edown_hbm,
    sgate_hbm,
    sup_hbm,
    sdown_hbm,
    out_ref,
    new_ref,
    new_filter_ref,
    tokens_ref,
    routes_ref,
    rweight_ref,
    mgain_ref,
    gate_ref,
    input_ref,
    step_ref,
    vecw_ref,
    bias_ref,
    rate_ref,
    jolt_ref,
    taps_ref,
    filter_ref,
    skip_ref,
    hgain_ref,
    outw_ref,
    cgain_ref,
    wgate_ref,
    wup_ref,
    wdown_ref,
    normed_buf,
    vec_out,
    vec_in,
    half_buf,
    column_buf,
    write_buf,
    part_buf,
    mix_buf,
    resid_buf,
    share_buf,
    acc_buf,
    hidden_buf,
    cross_out,
    cross_in,
    own_buf,
    term_buf,
    back_buf,
    load_sem,
    wide_sem,
    vec_send,
    vec_recv,
    mix_send,
    mix_recv,
    share_send,
    share_recv,
    resid_send,
    pass_send,
    resid_recv,
    cross_send,
    cross_recv,
    back_send,
    back_recv,
):
    ep = lax.axis_index("ep")
    tp = lax.axis_index("tp")
    core = lax.rem(tp, 2)
    z = tp // 2
    n_z = n_tp // 2
    n_same = n_ep * n_z
    partner = tp + 1 - 2 * core
    rows, model = tokens_ref.shape
    columns = out_ref.shape[1]
    heads = bias_ref.shape[1]
    width = gate_ref.shape[1]
    all_rows = n_ep * rows
    local = egate_hbm.shape[0]
    experts = local + 1
    units = wgate_ref.shape[-1]
    features = write_hbm.shape[0]
    group_lanes = GROUPS * STATE

    small = [
        (tokens_hbm, tokens_ref),
        (mgain_hbm, mgain_ref),
        (write_hbm, vecw_ref.at[:, :group_lanes]),
        (read_hbm, vecw_ref.at[:, group_lanes:]),
        (step_hbm, step_ref),
        (input_hbm, input_ref),
        (gate_hbm, gate_ref),
        (bias_hbm, bias_ref),
        (rate_hbm, rate_ref),
        (jolt_hbm, jolt_ref),
        (taps_hbm, taps_ref),
        (filter_hbm, filter_ref),
        (skip_hbm, skip_ref),
        (hgain_hbm, hgain_ref),
        (routes_hbm, routes_ref),
        (share_hbm, rweight_ref),
        (state_hbm, new_ref),
        (outw_hbm, outw_ref),
        (cgain_hbm, cgain_ref),
    ]
    loads = [
        pltpu.make_async_copy(src, dst, load_sem.at[i]) for i, (src, dst) in enumerate(small)
    ]
    wide = []
    for j in range(experts):
        for h in range(2):
            if j < local:
                wide.append((egate_hbm.at[j, :, h], wgate_ref.at[j, h]))
                wide.append((eup_hbm.at[j, :, h], wup_ref.at[j, h]))
            else:
                wide.append((sgate_hbm.at[:, h], wgate_ref.at[j, h]))
                wide.append((sup_hbm.at[:, h], wup_ref.at[j, h]))
    for j in range(experts):
        src = edown_hbm.at[j] if j < local else sdown_hbm
        wide.append((src, wdown_ref.at[pl.ds(j * units, units)]))
    wide = [pltpu.make_async_copy(src, dst, wide_sem.at[i]) for i, (src, dst) in enumerate(wide)]
    downs = wide[-experts:]
    ups = wide[:-experts]

    barrier = pltpu.get_barrier_semaphore()
    for k in range(1, n_tp):
        pl.semaphore_signal(
            barrier, inc=1, device_id=(ep, lax.rem(tp + k, n_tp)), device_id_type=MESH
        )
    for k in range(1, n_ep):
        pl.semaphore_signal(
            barrier, inc=1, device_id=(lax.rem(ep + k, n_ep), tp), device_id_type=MESH
        )
    for load in loads[:16]:
        load.start()

    def remote(src, dst, send, recv, device):
        return pltpu.make_async_remote_copy(
            src_ref=src,
            dst_ref=dst,
            send_sem=send,
            recv_sem=recv,
            device_id=device,
            device_id_type=MESH,
        )

    tp_order = [k for k in far_first(n_tp) if k]

    def tp_peer(k):
        return lax.rem(tp + k, n_tp)

    per_group = HEADS // GROUPS

    def vec_copy(k):
        peer = tp_peer(k)
        group = (peer * heads) // per_group
        return remote(
            vec_out.at[group], vec_in.at[tp], vec_send.at[k], vec_recv.at[tp], (ep, peer)
        )

    def vec_from(k):
        peer = tp_peer(k)
        return remote(
            vec_out.at[0], vec_in.at[peer], vec_send.at[k], vec_recv.at[peer], (ep, peer)
        )

    def share_copy(k):
        peer = lax.rem(ep + k, n_ep)
        return remote(
            share_buf.at[ep], share_buf.at[ep], share_send.at[k], share_recv.at[ep], (peer, tp)
        )

    def share_from(k):
        peer = lax.rem(ep + k, n_ep)
        return remote(
            share_buf.at[peer], share_buf.at[peer], share_send.at[k], share_recv.at[peer], (peer, tp)
        )

    def mix_copy(k):
        peer = tp_peer(k)
        return remote(
            part_buf.at[peer], mix_buf.at[tp], mix_send.at[k], mix_recv.at[tp], (ep, peer)
        )

    def mix_from(k):
        peer = tp_peer(k)
        return remote(
            part_buf.at[peer], mix_buf.at[peer], mix_send.at[k], mix_recv.at[peer], (ep, peer)
        )

    loads[0].wait()
    loads[1].wait()
    tokens = tokens_ref[...].astype(F32)
    scale = lax.rsqrt(jnp.mean(tokens * tokens, axis=-1, keepdims=True) + EPS)
    normed_buf[...] = (tokens * scale * mgain_ref[...]).astype(BF16)
    own = normed_buf[:, pl.ds(pl.multiple_of(tp * features, features), features)]
    loads[2].wait()
    loads[3].wait()
    vec_part = dot(own, vecw_ref[...]).astype(BF16)
    for g in range(GROUPS):
        at = slice(g * STATE, (g + 1) * STATE)
        vec_out[g, :, :STATE] = vec_part[:, at]
        vec_out[g, :, STATE:] = vec_part[:, group_lanes + g * STATE : group_lanes + (g + 1) * STATE]
    pl.semaphore_wait(barrier, n_tp - 1 + n_ep - 1)
    for k in tp_order:
        vec_copy(k).start()
    for load in loads[16:]:
        load.start()
    vec_in[tp] = vec_out[(tp * heads) // per_group]

    normed = normed_buf[...]
    loads[4].wait()
    step_raw = dot_nt(normed, step_ref[...])
    loads[5].wait()
    inputs = dot(normed, input_ref[...]).astype(BF16)
    loads[6].wait()
    gate_rows = dot(normed, gate_ref[...]).astype(BF16)
    for load in loads[7:16]:
        load.wait()
    taps = taps_ref[...].astype(F32)
    last = filter_ref.shape[0]
    total = inputs.astype(F32) * taps[last : last + 1]
    for i in range(last):
        total = total + filter_ref[i].astype(F32) * taps[i : i + 1]
        new_filter_ref[i] = filter_ref[i + 1] if i + 1 < last else inputs
    filtered = jax.nn.silu(total)
    jolt = jnp.transpose(
        jnp.concatenate([jolt_ref[...], jnp.zeros((heads, LANES - rows), F32)], axis=1)
    )[:rows]
    step = softplus(step_raw + bias_ref[...])
    decay = jnp.exp(jolt - jnp.exp(rate_ref[...]) * step)
    skip = jnp.broadcast_to(skip_ref[...], (rows, heads))
    stacked = jnp.concatenate([step, decay, skip], axis=0)
    head_lane = lax.broadcasted_iota(jnp.int32, (heads, width), 1) // HEAD_DIM
    spread = jnp.where(
        head_lane == lax.broadcasted_iota(jnp.int32, (heads, width), 0), 1.0, 0.0
    ).astype(BF16)
    high, low = split(stacked)
    expanded = dot(high, spread) + dot(low, spread)
    decay_row = expanded[rows : 2 * rows]
    x_row = expanded[:rows] * filtered
    direct = expanded[2 * rows :] * filtered
    gate_silu = jax.nn.silu(gate_rows.astype(F32))
    column_buf[...] = jnp.transpose(
        jnp.concatenate([x_row, decay_row, jnp.zeros((LANES - 2 * rows, width), F32)], axis=0)
    )

    ids = lax.broadcasted_iota(jnp.int32, (LANES, rows), 0)
    share = jnp.zeros((LANES, rows), F32)
    for k in range(routes_ref.shape[0]):
        share = share + jnp.where(
            routes_ref[k : k + 1, :] == ids, rweight_ref[k : k + 1, :], 0.0
        )
    share_buf[ep] = jnp.transpose(
        jnp.concatenate([share, jnp.zeros((LANES, LANES - rows), F32)], axis=1)
    )[:rows]
    for k in range(1, n_ep):
        share_copy(k).start()

    loads[16].wait()
    for s in range(rows):
        half_buf[:, s * STATE : (s + 1) * STATE] = new_ref[s].astype(BF16)

    for k in reversed(tp_order):
        vec_from(k).wait_recv()
    for load in ups:
        load.start()
    for load in downs:
        load.start()
    vecs = jax.nn.silu(jnp.sum(vec_in[...].astype(F32), axis=0))
    write = vecs[:, :STATE]
    read = vecs[:, STATE:]
    write_buf[...] = write
    row_ids = lax.broadcasted_iota(jnp.int32, (rows, STATE), 0)
    spread_read = jnp.concatenate(
        [jnp.where(row_ids == s, read, 0.0).astype(BF16) for s in range(rows)], axis=1
    )
    state_read = dot_nt(spread_read, half_buf[...])
    overlap = jnp.sum(write * read, axis=1, keepdims=True)
    value = (decay_row * state_read + x_row * overlap + direct) * gate_silu
    same = (
        lax.broadcasted_iota(jnp.int32, (LANES, LANES), 0) // HEAD_DIM
        == lax.broadcasted_iota(jnp.int32, (LANES, LANES), 1) // HEAD_DIM
    )
    block = jnp.where(same, 1.0 / HEAD_DIM, 0.0).astype(BF16)
    pieces = width // LANES
    square = (value * value).astype(BF16)
    means = dot(
        jnp.concatenate([square[:, j * LANES : (j + 1) * LANES] for j in range(pieces)], axis=0),
        block,
    )
    mean_square = jnp.concatenate(
        [means[j * rows : (j + 1) * rows] for j in range(pieces)], axis=1
    )
    gated = (value * lax.rsqrt(mean_square + EPS) * hgain_ref[...]).astype(BF16)
    loads[17].wait()

    def part_of(t):
        return dot(
            gated, outw_ref[:, pl.ds(pl.multiple_of(t * columns, columns), columns)]
        ).astype(BF16)

    for k in tp_order:
        peer = tp_peer(k)
        part_buf[peer] = part_of(peer)
        mix_copy(k).start()
    mix_buf[tp] = part_of(tp)

    for s in range(rows):
        new_ref[s] = (
            column_buf[:, rows + s : rows + s + 1] * new_ref[s]
            + column_buf[:, s : s + 1] * write_buf[s : s + 1, :]
        )

    own_tokens = tokens_ref[:, pl.ds(pl.multiple_of(tp * columns, columns), columns)]
    for k in reversed(tp_order):
        mix_from(k).wait_recv()
    mixed = jnp.sum(mix_buf[...].astype(F32), axis=0).astype(BF16)
    resid_buf[core, z, ep] = (own_tokens.astype(F32) + mixed.astype(F32)).astype(BF16)

    def place(m):
        return lax.rem(ep + m // n_z, n_ep), lax.rem(z + m % n_z, n_z)

    def resid_copy(m):
        e, zz = place(m)
        here = resid_buf.at[core, z, ep]
        return remote(
            here,
            here,
            resid_send.at[m],
            resid_recv.at[core, z * n_ep + ep],
            (e, zz * 2 + core),
        )

    def resid_from(m):
        e, zz = place(m)
        there = resid_buf.at[core, zz, e]
        return remote(
            there, there, resid_send.at[m], resid_recv.at[core, zz * n_ep + e], (e, zz * 2 + core)
        )

    def pass_copy(m):
        e, zz = place(m)
        there = resid_buf.at[core, zz, e]
        return remote(
            there, there, pass_send.at[m], resid_recv.at[core, zz * n_ep + e], (ep, partner)
        )

    def pass_from(m):
        e, zz = place(m)
        there = resid_buf.at[1 - core, zz, e]
        return remote(
            there, there, pass_send.at[m], resid_recv.at[1 - core, zz * n_ep + e], (ep, partner)
        )

    loop(1, n_same, lambda k: resid_copy(n_same - k).start())
    pass_copy(0).start()
    loads[18].wait()
    for k in range(1, n_ep):
        share_from(k).wait_recv()
    shares = share_buf[...].reshape(all_rows, LANES)
    all_lanes = lax.broadcasted_iota(jnp.int32, shares.shape, 1)
    own_rows = lax.broadcasted_iota(jnp.int32, (all_rows, 1), 0) // rows == ep
    scales = [
        jnp.sum(jnp.where(all_lanes == ep * local + j, shares, 0.0), axis=1, keepdims=True)
        for j in range(local)
    ] + [jnp.where(own_rows, 1.0, 0.0)]
    for load in ups:
        load.wait()

    def relay(m):
        resid_from(m).wait_recv()
        pass_copy(m).start()

    loop(1, n_same, relay)

    def half(h):
        square = jnp.zeros((all_rows, columns), F32)
        scaled = []
        for zz in range(n_z):
            part = resid_buf[h, zz].reshape(all_rows, columns).astype(F32)
            square = square + part * part
            at = pl.multiple_of((zz * 2 + h) * columns, columns)
            scaled.append((part * cgain_ref[:, pl.ds(at, columns)]).astype(BF16))
        scaled = jnp.concatenate(scaled, axis=1)
        sums = []
        for j in range(experts):
            for weights in (wgate_ref, wup_ref):
                sums.append(dot(scaled, weights[j, h].reshape(n_z * columns, units)))
        return square, sums

    square, sums = half(core)
    for i, value in enumerate(sums):
        acc_buf[i] = value
    loop(0, n_same, lambda m: pass_from(m).wait_recv())
    square_two, sums = half(1 - core)
    mean_square = jnp.sum(square + square_two, axis=-1, keepdims=True) * (1.0 / model)
    scale = lax.rsqrt(mean_square + EPS)
    for j in range(experts):
        gate = (acc_buf[2 * j] + sums[2 * j]) * scale
        up = (acc_buf[2 * j + 1] + sums[2 * j + 1]) * scale
        hidden_buf[:, j * units : (j + 1) * units] = (
            jax.nn.silu(gate) * up * scales[j]
        ).astype(BF16)
    for load in downs:
        load.wait()
    hidden = hidden_buf[...]

    def down_of(t):
        return dot(hidden, wdown_ref[:, pl.ds(pl.multiple_of(t * columns, columns), columns)])

    def cross_copy(zz):
        return remote(
            cross_out.at[zz], cross_in.at[zz], cross_send.at[zz], cross_recv.at[zz], (ep, partner)
        )

    z_order = [lax.rem(z + k, n_z) for k in far_first(n_z)]
    for zz in z_order:
        cross_out[zz] = down_of(zz * 2 + 1 - core).astype(BF16)
        cross_copy(zz).start()
    for zz in z_order:
        own_buf[zz] = down_of(zz * 2 + core)

    def back_copy(zz, e, m):
        return remote(
            term_buf.at[zz, e],
            back_buf.at[ep * n_z + z],
            back_send.at[m],
            back_recv.at[ep * n_z + z],
            (e, zz * 2 + core),
        )

    def back_from(m):
        e, zz = place(m)
        return remote(
            term_buf.at[zz, e],
            back_buf.at[e * n_z + zz],
            back_send.at[m],
            back_recv.at[e * n_z + zz],
            (e, zz * 2 + core),
        )

    for i, k in enumerate(far_first(n_z)):
        zz = z_order[i]
        cross_copy(zz).wait_recv()
        term_buf[zz] = (own_buf[zz] + cross_in[zz].astype(F32)).astype(BF16).reshape(
            n_ep, rows, columns
        )
        for step_ep in range(n_ep - 1, -1, -1):
            if k or step_ep:
                back_copy(zz, lax.rem(ep + step_ep, n_ep), step_ep * n_z + k).start()
    back_buf[ep * n_z + z] = term_buf[z, ep]
    loop(1, n_same, lambda m: back_from(m).wait_recv())
    out_ref[...] = (
        resid_buf[core, z, ep].astype(F32) + jnp.sum(back_buf[...].astype(F32), axis=0)
    ).astype(BF16)

    for k in tp_order:
        vec_copy(k).wait_send()
        mix_copy(k).wait_send()
    for k in range(1, n_ep):
        share_copy(k).wait_send()
    loop(1, n_same, lambda m: resid_copy(m).wait_send())
    loop(0, n_same, lambda m: pass_copy(m).wait_send())
    for zz in range(n_z):
        cross_copy(zz).wait_send()
    loop(1, n_same, lambda m: back_from(m).wait_send())


def finish_kernel(out_in, new_in, filter_in, out_ref, new_ref, filter_ref, sem):
    pairs = ((new_in, new_ref), (out_in, out_ref), (filter_in, filter_ref))
    copies = [pltpu.make_async_copy(src, dst, sem.at[i]) for i, (src, dst) in enumerate(pairs)]
    for copy in copies:
        copy.start()
    for copy in copies:
        copy.wait()


def on_device(
    tokens,
    routes,
    route_weight,
    mixer_gain,
    gate_weight,
    input_weight,
    step_weight,
    write_weight,
    read_weight,
    step_bias,
    decay_log,
    decay_jolt,
    filter_taps,
    filter_state,
    scan_state,
    skip_gain,
    head_gain,
    output_weight,
    channel_gain,
    expert_gate,
    expert_up,
    expert_down,
    shared_gate,
    shared_up,
    shared_down,
):
    rows, model = tokens.shape
    n_tp = lax.axis_size("tp")
    n_ep = lax.axis_size("ep")
    n_z = n_tp // 2
    n_same = n_ep * n_z
    columns = model // n_tp
    heads_here = step_bias.shape[0]
    width = gate_weight.shape[1]
    local, _, units = expert_gate.shape
    experts = local + 1
    taps = filter_state.shape[1]
    hbm = pl.BlockSpec(memory_space=pl.ANY)
    vmem = pl.BlockSpec(memory_space=pltpu.VMEM)
    dma = pltpu.SemaphoreType.DMA
    shape = jax.ShapeDtypeStruct
    outs = (
        shape((rows, columns), BF16),
        shape((rows, width, STATE), F32),
        shape((taps, rows, width), BF16),
    )
    operands = (
        tokens,
        routes.T,
        route_weight.T,
        mixer_gain.reshape(1, model),
        gate_weight,
        input_weight,
        step_weight.T,
        write_weight,
        read_weight,
        step_bias.reshape(1, heads_here),
        decay_log.reshape(1, heads_here),
        decay_jolt.T,
        filter_taps,
        jnp.transpose(filter_state, (1, 0, 2)),
        scan_state.reshape(rows, width, STATE),
        skip_gain.reshape(1, heads_here),
        head_gain.reshape(1, width),
        output_weight,
        channel_gain.reshape(1, model),
        expert_gate.reshape(local, n_z, 2, columns, units),
        expert_up.reshape(local, n_z, 2, columns, units),
        expert_down,
        shared_gate.reshape(n_z, 2, columns, units),
        shared_up.reshape(n_z, 2, columns, units),
        shared_down,
    )
    vm = pltpu.VMEM
    held = [
        vm(operands[0].shape, BF16),
        vm(operands[1].shape, jnp.int32),
        vm(operands[2].shape, F32),
        vm(operands[3].shape, F32),
        vm(gate_weight.shape, BF16),
        vm(input_weight.shape, BF16),
        vm(operands[6].shape, BF16),
        vm((write_weight.shape[0], 2 * GROUPS * STATE), BF16),
        vm((1, heads_here), F32),
        vm((1, heads_here), F32),
        vm(operands[11].shape, F32),
        vm(filter_taps.shape, BF16),
        vm(operands[13].shape, BF16),
        vm((1, heads_here), F32),
        vm((1, width), F32),
        vm(output_weight.shape, BF16),
        vm((1, model), F32),
        vm((experts, 2, n_z, columns, units), BF16),
        vm((experts, 2, n_z, columns, units), BF16),
        vm((experts * units, model), BF16),
    ]
    layer_out, new_state, new_filter = pl.pallas_call(
        functools.partial(layer_kernel, n_ep, n_tp),
        out_shape=tuple(vm(out.shape, out.dtype) for out in outs),
        in_specs=[hbm] * len(operands),
        out_specs=(vmem,) * 3,
        scratch_shapes=held
        + [
            vm((rows, model), BF16),
            vm((GROUPS, rows, 2 * STATE), BF16),
            vm((n_tp, rows, 2 * STATE), BF16),
            vm((width, rows * STATE), BF16),
            vm((width, LANES), F32),
            vm((rows, STATE), F32),
            vm((n_tp, rows, columns), BF16),
            vm((n_tp, rows, columns), BF16),
            vm((2, n_z, n_ep, rows, columns), BF16),
            vm((n_ep, rows, LANES), F32),
            vm((2 * experts, n_ep * rows, units), F32),
            vm((n_ep * rows, experts * units), BF16),
            vm((n_z, n_ep * rows, columns), BF16),
            vm((n_z, n_ep * rows, columns), BF16),
            vm((n_z, n_ep * rows, columns), F32),
            vm((n_z, n_ep, rows, columns), BF16),
            vm((n_same, rows, columns), BF16),
            dma((19,)),
            dma((5 * experts,)),
            dma((n_tp,)),
            dma((n_tp,)),
            dma((n_tp,)),
            dma((n_tp,)),
            dma((n_ep,)),
            dma((n_ep,)),
            dma((n_same,)),
            dma((n_same,)),
            dma((2, n_same)),
            dma((n_z,)),
            dma((n_z,)),
            dma((n_same,)),
            dma((n_same,)),
        ],
        compiler_params=pltpu.CompilerParams(
            collective_id=0,
            has_side_effects=True,
            vmem_limit_bytes=VMEM_LIMIT - 4 * rows * width * STATE - SPARE,
        ),
        name="layer",
    )(*operands)
    layer_out, new_state, new_filter = pl.pallas_call(
        finish_kernel,
        out_shape=outs,
        in_specs=[vmem] * 3,
        out_specs=(hbm,) * 3,
        scratch_shapes=[dma((3,))],
        compiler_params=pltpu.CompilerParams(vmem_limit_bytes=1024 * 1024),
        name="finish",
    )(layer_out, new_state, new_filter)
    return (
        layer_out,
        new_state.reshape(scan_state.shape),
        jnp.transpose(new_filter, (1, 0, 2)),
    )


def solution(mesh):
    in_specs = (
        P("ep", None),
        P("ep", None),
        P("ep", None),
        P(),
        P(None, "tp"),
        P(None, "tp"),
        P(None, "tp"),
        P("tp", None),
        P("tp", None),
        P("tp"),
        P("tp"),
        P("ep", "tp"),
        P(None, "tp"),
        P("ep", None, "tp"),
        P("ep", "tp", None, None),
        P("tp"),
        P("tp"),
        P("tp", None),
        P(),
        P("ep", None, "tp"),
        P("ep", None, "tp"),
        P("ep", "tp", None),
        P(None, "tp"),
        P(None, "tp"),
        P("tp", None),
    )
    out_specs = (P("ep", "tp"), P("ep", "tp", None, None), P("ep", None, "tp"))
    return jax.shard_map(
        on_device, mesh=mesh, in_specs=in_specs, out_specs=out_specs, check_vma=False
    )
```

time: 50.5 us -> 32.6 us (0.65)
  the two profiles are of different devices: /device:TPU:25 before, /device:TPU:0 now
where the time goes in v1:
time: 32.6 us; the launch traced here: 32.4 us
  Pallas kernels  31.8 us (98%)
  between operations  0.65 us (2%)
    pallas_call x1, Pallas kernels, on_device(): pl.pallas_call(functools.partial(layer_kernel, n_ep, n_tp), out_shape=tup...  29.7 us
    pallas_call x1, Pallas kernels, on_device(): pl.pallas_call(finish_kernel, out_shape=outs, in_specs=[vmem] * 3, out_sp...  2.05 us

profile of v1, /device:TPU:0, one launch (start us, length us, event | category | flops | bytes accessed | tf_op | source)
XLA Modules:
  0.0 32.4 jit_solution(16131223577550805772)
XLA Ops:
  0.6 29.7 %layer.1 = (bf16[16,256]{1,0:T(8,128)(2,1)S(1)}, f32[16,512,128]{2,1,0:T(8,128)S(1)}, bf16[3,16,512]{2,1,0:T(8,128)(2,1)S(1)}) custom-call(bf16[16,2048]{1,0:T(8,128)(2,1)} %tokens_hbm.1, s32[4,16]{1,0:T(4,128)} %bitcast.28, f32[4,16]{1,0:T(4,128)} %bitcast.29, f32[1,2048]{1,0:T(1,128)} %bitcast.25, bf16[2048,512]{1,0:T(8,128)(2,1)} %gate_hbm.1, ...), custom_call_target="tpu_custom_call" | custom-call | tf_op jit(solution)/shard_map/layer/pallas_call | solution.py:651
  30.4 2.0 %finish.1 = (bf16[16,256]{1,0:T(8,128)(2,1)}, f32[16,512,128]{2,1,0:T(8,128)}, bf16[3,16,512]{2,1,0:T(8,128)(2,1)}) custom-call(bf16[16,256]{1,0:T(8,128)(2,1)S(1)} %get-tuple-element.9.out_in, f32[16,512,128]{2,1,0:T(8,128)S(1)} %get-tuple-element.10.new_in, bf16[3,16,512]{2,1,0:T(8,128)(2,1)S(1)} %get-tuple-element.11.filter_in), custom_call_target="tpu_custom_call" | custom-call | tf_op jit(solution)/shard_map/finish/pallas_call | solution.py:698

commit v2 on v1

v2 whole, which is shorter than its diff:
```python
import functools

import jax
import jax.numpy as jnp
from jax import lax
from jax.experimental import pallas as pl
from jax.experimental.pallas import tpu as pltpu
from jax.sharding import PartitionSpec as P

HEADS = 64
HEAD_DIM = 64
GROUPS = 4
STATE = 128

EPS = 1e-06
F32 = jnp.float32
BF16 = jnp.bfloat16
MESH = pl.DeviceIdType.MESH
VMEM_LIMIT = 67043328
SPARE = 64 * 1024
LANES = 128


def dot(a, b):
    return jnp.dot(a, b, preferred_element_type=F32)


def dot_nt(a, b):
    return lax.dot_general(a, b, (((1,), (1,)), ((), ())), preferred_element_type=F32)


def split(v):
    high = v.astype(BF16)
    return high, (v - high.astype(F32)).astype(BF16)


def softplus(v):
    return jnp.maximum(v, 0.0) + jnp.log1p(jnp.exp(-jnp.abs(v)))


def far_first(n):
    return sorted(range(n), key=lambda k: -min(k, n - k))


def layer_kernel(
    n_ep,
    n_tp,
    tokens_hbm,
    routes_hbm,
    share_hbm,
    mgain_hbm,
    gate_hbm,
    input_hbm,
    step_hbm,
    write_hbm,
    read_hbm,
    bias_hbm,
    rate_hbm,
    jolt_hbm,
    taps_hbm,
    filter_hbm,
    state_hbm,
    skip_hbm,
    hgain_hbm,
    outw_hbm,
    cgain_hbm,
    egate_hbm,
    eup_hbm,
    edown_hbm,
    sgate_hbm,
    sup_hbm,
    sdown_hbm,
    out_ref,
    new_ref,
    new_filter_ref,
    tokens_ref,
    routes_ref,
    rweight_ref,
    mgain_ref,
    gate_ref,
    input_ref,
    step_ref,
    vecw_ref,
    bias_ref,
    rate_ref,
    jolt_ref,
    taps_ref,
    filter_ref,
    skip_ref,
    hgain_ref,
    outw_ref,
    cgain_ref,
    wide_ref,
    down_ref,
    normed_buf,
    vec_out,
    vec_in,
    half_buf,
    column_buf,
    write_buf,
    part_buf,
    mix_in,
    resid_buf,
    share_buf,
    acc_buf,
    hidden_buf,
    cross_out,
    cross_in,
    own_buf,
    term_buf,
    back_in,
    load_sem,
    send_sem,
    recv_sem,
    direct_recv,
    pass_recv,
    cross_recv,
):
    ep = lax.axis_index("ep")
    tp = lax.axis_index("tp")
    core = lax.rem(tp, 2)
    z = tp // 2
    n_z = n_tp // 2
    n_same = n_ep * n_z
    partner = tp + 1 - 2 * core
    rows, model = tokens_ref.shape
    columns = out_ref.shape[1]
    heads = bias_ref.shape[1]
    width = gate_ref.shape[1]
    all_rows = n_ep * rows
    local = egate_hbm.shape[0]
    experts = local + 1
    units = edown_hbm.shape[1]
    features = write_hbm.shape[0]
    group_lanes = GROUPS * STATE
    per_group = HEADS // GROUPS
    tp_order = [k for k in far_first(n_tp) if k] + [0]
    z_far = far_first(n_z)
    z_near = z_far[::-1]

    def tp_peer(k):
        return lax.rem(tp + k, n_tp)

    def ep_peer(k):
        return lax.rem(ep + k, n_ep)

    def z_peer(k):
        return lax.rem(z + k, n_z)

    def block(t, size):
        return pl.ds(pl.multiple_of(t * size, size), size)

    def loaded(i, dst):
        return pltpu.make_async_copy(dst, dst, load_sem.at[i])

    singles = [
        (tokens_hbm, tokens_ref),
        (mgain_hbm, mgain_ref),
        (write_hbm, vecw_ref.at[:, :group_lanes]),
        (read_hbm, vecw_ref.at[:, group_lanes:]),
        (step_hbm, step_ref),
        (input_hbm, input_ref),
        (gate_hbm, gate_ref),
        (bias_hbm, bias_ref),
        (rate_hbm, rate_ref),
        (jolt_hbm, jolt_ref),
        (taps_hbm, taps_ref),
        (filter_hbm, filter_ref),
        (skip_hbm, skip_ref),
        (hgain_hbm, hgain_ref),
        (routes_hbm, routes_ref),
        (share_hbm, rweight_ref),
        (state_hbm, new_ref),
        (cgain_hbm, cgain_ref),
    ]
    loads = [
        pltpu.make_async_copy(src, dst, load_sem.at[i if i != 3 else 2])
        for i, (src, dst) in enumerate(singles)
    ]
    outw_sem, wide_sem, down_sem = 3, 18, 19
    outw_loads = [
        pltpu.make_async_copy(
            outw_hbm.at[:, block(tp_peer(k), columns)],
            outw_ref.at[:, i * columns : (i + 1) * columns],
            load_sem.at[outw_sem],
        )
        for i, k in enumerate(tp_order)
    ]
    wide_loads = []
    for side in range(2):
        for k in z_near:
            t = z_peer(k) * 2 + (1 - core if side == 0 else core)
            for j in range(experts):
                for g, (routed, shared) in enumerate(
                    ((egate_hbm, sgate_hbm), (eup_hbm, sup_hbm))
                ):
                    source = routed.at[j] if j < local else shared
                    lane = (2 * j + g) * units
                    wide_loads.append(
                        pltpu.make_async_copy(
                            source.at[block(t, columns)],
                            wide_ref.at[side, k, :, lane : lane + units],
                            load_sem.at[wide_sem],
                        )
                    )
    down_loads = []
    for side in range(2):
        for i, k in enumerate(z_far):
            t = z_peer(k) * 2 + (core if side == 0 else 1 - core)
            for j in range(experts):
                source = edown_hbm.at[j] if j < local else sdown_hbm
                down_loads.append(
                    pltpu.make_async_copy(
                        source.at[:, block(t, columns)],
                        down_ref.at[
                            side,
                            j * units : (j + 1) * units,
                            i * columns : (i + 1) * columns,
                        ],
                        load_sem.at[down_sem],
                    )
                )

    barrier = pltpu.get_barrier_semaphore()
    for k in range(1, n_tp):
        pl.semaphore_signal(barrier, inc=1, device_id=(ep, tp_peer(k)), device_id_type=MESH)
    for k in range(1, n_ep):
        pl.semaphore_signal(barrier, inc=1, device_id=(ep_peer(k), tp), device_id_type=MESH)
    for load in loads[:16]:
        load.start()

    def remote(src, dst, send, recv, device):
        return pltpu.make_async_remote_copy(
            src_ref=src,
            dst_ref=dst,
            send_sem=send_sem.at[send],
            recv_sem=recv,
            device_id=device,
            device_id_type=MESH,
        )

    VEC, SHARE, MIX, RESID, PASS, CROSS, BACK = range(7)
    vec_recv, share_recv, mix_recv, back_recv = (recv_sem.at[i] for i in range(4))

    def vec_copy(k):
        peer = tp_peer(k)
        group = (peer * heads) // per_group
        return remote(vec_out.at[group], vec_in.at[k - 1], VEC, vec_recv, (ep, peer))

    def share_copy(k):
        target = (lax.rem(ep + n_ep - k, n_ep), tp)
        return remote(share_buf.at[0], share_buf.at[k], SHARE, share_recv, target)

    def mix_copy(i, k):
        return remote(part_buf.at[i], mix_in.at[k - 1], MIX, mix_recv, (ep, tp_peer(k)))

    def resid_copy(e, k):
        here = resid_buf.at[1, 0, 0]
        target = (lax.rem(ep + n_ep - e, n_ep), lax.rem(z + n_z - k, n_z) * 2 + 1 - core)
        return remote(here, resid_buf.at[0, k, e], RESID, direct_recv.at[k], target)

    def pass_copy(k):
        at = pl.ds(0 if k else 1, n_ep if k else n_ep - 1)
        return remote(
            resid_buf.at[0, k, at], resid_buf.at[1, k, at], PASS, pass_recv.at[k], (ep, partner)
        )

    half_z = n_z // 2

    def cross_copy(i):
        at = pl.ds(i * half_z, half_z)
        return remote(cross_out.at[at], cross_in.at[at], CROSS, cross_recv.at[i], (ep, partner))

    def back_copy(i, e, k):
        target = (ep_peer(e), z_peer(k) * 2 + 1 - core)
        return remote(term_buf.at[i, e], back_in.at[e * n_z + k], BACK, back_recv, target)

    def whole(buf, send, recv):
        return remote(buf, buf, send, recv, (ep, partner))

    loads[0].wait()
    loads[1].wait()
    tokens = tokens_ref[...].astype(F32)
    scale = lax.rsqrt(jnp.mean(tokens * tokens, axis=-1, keepdims=True) + EPS)
    normed_buf[...] = (tokens * scale * mgain_ref[...]).astype(BF16)
    own = normed_buf[:, block(tp, features)]
    loaded(2, vecw_ref).wait()
    vec_part = dot(own, vecw_ref[...]).astype(BF16)
    for g in range(GROUPS):
        at = slice(g * STATE, (g + 1) * STATE)
        vec_out[g, :, :STATE] = vec_part[:, at]
        vec_out[g, :, STATE:] = vec_part[:, group_lanes + g * STATE : group_lanes + (g + 1) * STATE]
    pl.semaphore_wait(barrier, n_tp - 1 + n_ep - 1)
    for k in tp_order[:-1]:
        vec_copy(k).start()
    loads[16].start()
    for load in outw_loads:
        load.start()
    loads[17].start()

    normed = normed_buf[...]
    loads[4].wait()
    step_raw = dot_nt(normed, step_ref[...])
    loads[5].wait()
    inputs = dot(normed, input_ref[...]).astype(BF16)
    loads[6].wait()
    gate_rows = dot(normed, gate_ref[...]).astype(BF16)
    for load in loads[7:16]:
        load.wait()
    taps = taps_ref[...].astype(F32)
    last = filter_ref.shape[0]
    total = inputs.astype(F32) * taps[last : last + 1]
    for i in range(last):
        total = total + filter_ref[i].astype(F32) * taps[i : i + 1]
        new_filter_ref[i] = filter_ref[i + 1] if i + 1 < last else inputs
    filtered = jax.nn.silu(total)
    jolt = jnp.transpose(
        jnp.concatenate([jolt_ref[...], jnp.zeros((heads, LANES - rows), F32)], axis=1)
    )[:rows]
    step = softplus(step_raw + bias_ref[...])
    decay = jnp.exp(jolt - jnp.exp(rate_ref[...]) * step)
    skip = jnp.broadcast_to(skip_ref[...], (rows, heads))
    stacked = jnp.concatenate([step, decay, skip], axis=0)
    head_lane = lax.broadcasted_iota(jnp.int32, (heads, width), 1) // HEAD_DIM
    spread = jnp.where(
        head_lane == lax.broadcasted_iota(jnp.int32, (heads, width), 0), 1.0, 0.0
    ).astype(BF16)
    high, low = split(stacked)
    expanded = dot(high, spread) + dot(low, spread)
    decay_row = expanded[rows : 2 * rows]
    x_row = expanded[:rows] * filtered
    direct = expanded[2 * rows :] * filtered
    gate_silu = jax.nn.silu(gate_rows.astype(F32))
    column_buf[...] = jnp.transpose(
        jnp.concatenate([x_row, decay_row, jnp.zeros((LANES - 2 * rows, width), F32)], axis=0)
    )

    ids = lax.broadcasted_iota(jnp.int32, (LANES, rows), 0)
    share = jnp.zeros((LANES, rows), F32)
    for k in range(routes_ref.shape[0]):
        share = share + jnp.where(
            routes_ref[k : k + 1, :] == ids, rweight_ref[k : k + 1, :], 0.0
        )
    share_buf[0] = jnp.transpose(
        jnp.concatenate([share, jnp.zeros((LANES, LANES - rows), F32)], axis=1)
    )[:rows]
    for k in range(1, n_ep):
        share_copy(k).start()

    loads[16].wait()
    for s in range(rows):
        half_buf[:, s * STATE : (s + 1) * STATE] = new_ref[s].astype(BF16)

    for load in wide_loads:
        load.start()
    for load in down_loads:
        load.start()
    whole(vec_in, VEC, vec_recv).wait_recv()
    vecs = jax.nn.silu(
        vec_out[(tp * heads) // per_group].astype(F32)
        + jnp.sum(vec_in[...].astype(F32), axis=0)
    )
    write = vecs[:, :STATE]
    read = vecs[:, STATE:]
    write_buf[...] = write
    row_ids = lax.broadcasted_iota(jnp.int32, (rows, STATE), 0)
    spread_read = jnp.concatenate(
        [jnp.where(row_ids == s, read, 0.0).astype(BF16) for s in range(rows)], axis=1
    )
    state_read = dot_nt(spread_read, half_buf[...])
    overlap = jnp.sum(write * read, axis=1, keepdims=True)
    value = (decay_row * state_read + x_row * overlap + direct) * gate_silu
    same = (
        lax.broadcasted_iota(jnp.int32, (LANES, LANES), 0) // HEAD_DIM
        == lax.broadcasted_iota(jnp.int32, (LANES, LANES), 1) // HEAD_DIM
    )
    averaging = jnp.where(same, 1.0 / HEAD_DIM, 0.0).astype(BF16)
    pieces = width // LANES
    square = (value * value).astype(BF16)
    means = dot(
        jnp.concatenate([square[:, j * LANES : (j + 1) * LANES] for j in range(pieces)], axis=0),
        averaging,
    )
    mean_square = jnp.concatenate(
        [means[j * rows : (j + 1) * rows] for j in range(pieces)], axis=1
    )
    gated = (value * lax.rsqrt(mean_square + EPS) * hgain_ref[...]).astype(BF16)
    loaded(outw_sem, outw_ref).wait()
    half_tp = n_tp // 2
    for h in range(2):
        at = slice(h * half_tp * columns, (h + 1) * half_tp * columns)
        part = dot(gated, outw_ref[:, at]).astype(BF16)
        for i in range(half_tp):
            part_buf[h * half_tp + i] = part[:, i * columns : (i + 1) * columns]
        for i in range(half_tp):
            k = tp_order[h * half_tp + i]
            if k:
                mix_copy(h * half_tp + i, k).start()

    for s in range(rows):
        new_ref[s] = (
            column_buf[:, rows + s : rows + s + 1] * new_ref[s]
            + column_buf[:, s : s + 1] * write_buf[s : s + 1, :]
        )

    own_mix = tokens_ref[:, block(tp, columns)].astype(F32)
    whole(mix_in, MIX, mix_recv).wait_recv()
    mixed = (
        part_buf[n_tp - 1].astype(F32) + jnp.sum(mix_in[...].astype(F32), axis=0)
    ).astype(BF16)
    resid_buf[1, 0, 0] = (own_mix + mixed.astype(F32)).astype(BF16)
    for k in z_near:
        for e in range(n_ep - 1, -1, -1):
            resid_copy(e, k).start()

    loads[17].wait()
    whole(share_buf.at[pl.ds(1, n_ep - 1)], SHARE, share_recv).wait_recv()
    shares = share_buf[...].reshape(all_rows, LANES)
    all_lanes = lax.broadcasted_iota(jnp.int32, shares.shape, 1)
    own_rows = lax.broadcasted_iota(jnp.int32, (all_rows, 1), 0) < rows
    scales = [
        jnp.sum(jnp.where(all_lanes == ep * local + j, shares, 0.0), axis=1, keepdims=True)
        for j in range(local)
    ] + [jnp.where(own_rows, 1.0, 0.0)]
    loaded(wide_sem, wide_ref).wait()
    loaded(down_sem, down_ref).wait()

    squares = []

    def piece(side, k):
        part = resid_buf[side, k].reshape(all_rows, columns).astype(F32)
        squares.append(part * part)
        t = z_peer(k) * 2 + (1 - core if side == 0 else core)
        scaled = (part * cgain_ref[:, block(t, columns)]).astype(BF16)
        product = dot(scaled, wide_ref[side, k])
        if len(squares) == 1:
            acc_buf[...] = product
        else:
            acc_buf[...] += product

    def relay(k):
        whole(resid_buf.at[0, k], RESID, direct_recv.at[k]).wait_recv()
        pass_copy(k).start()
        piece(0, k)

    def passed(k):
        pass_copy(k).wait_recv()
        piece(1, k)

    for k in z_near[:-1]:
        relay(k)
    passed(z_near[0])
    relay(z_near[-1])
    for k in z_near[1:]:
        passed(k)
    square = squares[0]
    for other in squares[1:]:
        square = square + other
    scale = lax.rsqrt(jnp.sum(square, axis=-1, keepdims=True) * (1.0 / model) + EPS)
    for j in range(experts):
        gate = acc_buf[:, 2 * j * units : (2 * j + 1) * units] * scale
        up = acc_buf[:, (2 * j + 1) * units : (2 * j + 2) * units] * scale
        hidden_buf[:, j * units : (j + 1) * units] = (
            jax.nn.silu(gate) * up * scales[j]
        ).astype(BF16)
    hidden = hidden_buf[...]
    span = half_z * columns
    for h in range(2):
        result = dot(hidden, down_ref[0, :, h * span : (h + 1) * span]).astype(BF16)
        for i in range(half_z):
            cross_out[h * half_z + i] = result[:, i * columns : (i + 1) * columns]
        cross_copy(h).start()
    result = dot(hidden, down_ref[1])
    for i in range(n_z):
        own_buf[i] = result[:, i * columns : (i + 1) * columns]
    for h in range(2):
        cross_copy(h).wait_recv()
        for i in range(h * half_z, (h + 1) * half_z):
            k = z_far[i]
            term_buf[i] = (
                (own_buf[i] + cross_in[i].astype(F32)).astype(BF16).reshape(n_ep, rows, columns)
            )
            for e in range(n_ep - 1, -1, -1):
                back_copy(i, e, k).start()
    whole(back_in, BACK, back_recv).wait_recv()
    out_ref[...] = (
        resid_buf[1, 0, 0].astype(F32) + jnp.sum(back_in[...].astype(F32), axis=0)
    ).astype(BF16)

    whole(vec_in, VEC, vec_recv).wait_send()
    whole(share_buf.at[pl.ds(1, n_ep - 1)], SHARE, share_recv).wait_send()
    whole(mix_in, MIX, mix_recv).wait_send()
    whole(back_in, RESID, back_recv).wait_send()
    for k in range(n_z):
        pass_copy(k).wait_send()
    whole(cross_out, CROSS, back_recv).wait_send()
    whole(back_in, BACK, back_recv).wait_send()


def finish_kernel(out_in, new_in, filter_in, out_ref, new_ref, filter_ref, sem):
    pairs = ((new_in, new_ref), (out_in, out_ref), (filter_in, filter_ref))
    copies = [pltpu.make_async_copy(src, dst, sem.at[i]) for i, (src, dst) in enumerate(pairs)]
    for copy in copies:
        copy.start()
    for copy in copies:
        copy.wait()


def on_device(
    tokens,
    routes,
    route_weight,
    mixer_gain,
    gate_weight,
    input_weight,
    step_weight,
    write_weight,
    read_weight,
    step_bias,
    decay_log,
    decay_jolt,
    filter_taps,
    filter_state,
    scan_state,
    skip_gain,
    head_gain,
    output_weight,
    channel_gain,
    expert_gate,
    expert_up,
    expert_down,
    shared_gate,
    shared_up,
    shared_down,
):
    rows, model = tokens.shape
    n_tp = lax.axis_size("tp")
    n_ep = lax.axis_size("ep")
    n_z = n_tp // 2
    n_same = n_ep * n_z
    columns = model // n_tp
    heads_here = step_bias.shape[0]
    width = gate_weight.shape[1]
    local, _, units = expert_gate.shape
    experts = local + 1
    taps = filter_state.shape[1]
    hbm = pl.BlockSpec(memory_space=pl.ANY)
    vmem = pl.BlockSpec(memory_space=pltpu.VMEM)
    dma = pltpu.SemaphoreType.DMA
    shape = jax.ShapeDtypeStruct
    outs = (
        shape((rows, columns), BF16),
        shape((rows, width, STATE), F32),
        shape((taps, rows, width), BF16),
    )
    operands = (
        tokens,
        routes.T,
        route_weight.T,
        mixer_gain.reshape(1, model),
        gate_weight,
        input_weight,
        step_weight.T,
        write_weight,
        read_weight,
        step_bias.reshape(1, heads_here),
        decay_log.reshape(1, heads_here),
        decay_jolt.T,
        filter_taps,
        jnp.transpose(filter_state, (1, 0, 2)),
        scan_state.reshape(rows, width, STATE),
        skip_gain.reshape(1, heads_here),
        head_gain.reshape(1, width),
        output_weight,
        channel_gain.reshape(1, model),
        expert_gate,
        expert_up,
        expert_down,
        shared_gate,
        shared_up,
        shared_down,
    )
    vm = pltpu.VMEM
    held = [
        vm(operands[0].shape, BF16),
        vm(operands[1].shape, jnp.int32),
        vm(operands[2].shape, F32),
        vm(operands[3].shape, F32),
        vm(gate_weight.shape, BF16),
        vm(input_weight.shape, BF16),
        vm(operands[6].shape, BF16),
        vm((write_weight.shape[0], 2 * GROUPS * STATE), BF16),
        vm((1, heads_here), F32),
        vm((1, heads_here), F32),
        vm(operands[11].shape, F32),
        vm(filter_taps.shape, BF16),
        vm(operands[13].shape, BF16),
        vm((1, heads_here), F32),
        vm((1, width), F32),
        vm(output_weight.shape, BF16),
        vm((1, model), F32),
        vm((2, n_z, columns, 2 * experts * units), BF16),
        vm((2, experts * units, n_z * columns), BF16),
    ]
    layer_out, new_state, new_filter = pl.pallas_call(
        functools.partial(layer_kernel, n_ep, n_tp),
        out_shape=tuple(vm(out.shape, out.dtype) for out in outs),
        in_specs=[hbm] * len(operands),
        out_specs=(vmem,) * 3,
        scratch_shapes=held
        + [
            vm((rows, model), BF16),
            vm((GROUPS, rows, 2 * STATE), BF16),
            vm((n_tp - 1, rows, 2 * STATE), BF16),
            vm((width, rows * STATE), BF16),
            vm((width, LANES), F32),
            vm((rows, STATE), F32),
            vm((n_tp, rows, columns), BF16),
            vm((n_tp - 1, rows, columns), BF16),
            vm((2, n_z, n_ep, rows, columns), BF16),
            vm((n_ep, rows, LANES), F32),
            vm((n_ep * rows, 2 * experts * units), F32),
            vm((n_ep * rows, experts * units), BF16),
            vm((n_z, n_ep * rows, columns), BF16),
            vm((n_z, n_ep * rows, columns), BF16),
            vm((n_z, n_ep * rows, columns), F32),
            vm((n_z, n_ep, rows, columns), BF16),
            vm((n_same, rows, columns), BF16),
            dma((20,)),
            dma((7,)),
            dma((4,)),
            dma((n_z,)),
            dma((n_z,)),
            dma((2,)),
        ],
        compiler_params=pltpu.CompilerParams(
            collective_id=0,
            has_side_effects=True,
            vmem_limit_bytes=VMEM_LIMIT - 4 * rows * width * STATE - SPARE,
        ),
        name="layer",
    )(*operands)
    layer_out, new_state, new_filter = pl.pallas_call(
        finish_kernel,
        out_shape=outs,
        in_specs=[vmem] * 3,
        out_specs=(hbm,) * 3,
        scratch_shapes=[dma((3,))],
        compiler_params=pltpu.CompilerParams(vmem_limit_bytes=1024 * 1024),
        name="finish",
    )(layer_out, new_state, new_filter)
    return (
        layer_out,
        new_state.reshape(scan_state.shape),
        jnp.transpose(new_filter, (1, 0, 2)),
    )


def solution(mesh):
    in_specs = (
        P("ep", None),
        P("ep", None),
        P("ep", None),
        P(),
        P(None, "tp"),
        P(None, "tp"),
        P(None, "tp"),
        P("tp", None),
        P("tp", None),
        P("tp"),
        P("tp"),
        P("ep", "tp"),
        P(None, "tp"),
        P("ep", None, "tp"),
        P("ep", "tp", None, None),
        P("tp"),
        P("tp"),
        P("tp", None),
        P(),
        P("ep", None, "tp"),
        P("ep", None, "tp"),
        P("ep", "tp", None),
        P(None, "tp"),
        P(None, "tp"),
        P("tp", None),
    )
    out_specs = (P("ep", "tp"), P("ep", "tp", None, None), P("ep", None, "tp"))
    return jax.shard_map(
        on_device, mesh=mesh, in_specs=in_specs, out_specs=out_specs, check_vma=False
    )
```

time: 32.6 us -> 29.7 us (0.911)
  Pallas kernels: 31.8 us -> 29 us
    pallas_call x1, Pallas kernels: 29.7 us -> 26.9 us  [on_device(): pl.pallas_call(functools.partial(layer_kernel, n_ep, n_tp), out_shape=tup...]
where the time goes in v2:
time: 29.7 us; the launch traced here: 29.6 us
  Pallas kernels  29 us (98%)
  between operations  0.65 us (2%)
    pallas_call x1, Pallas kernels, on_device(): pl.pallas_call(functools.partial(layer_kernel, n_ep, n_tp), out_shape=tup...  26.9 us
    pallas_call x1, Pallas kernels, on_device(): pl.pallas_call(finish_kernel, out_shape=outs, in_specs=[vmem] * 3, out_sp...  2.05 us

profile of v2, /device:TPU:0, one launch (start us, length us, event | category | flops | bytes accessed | tf_op | source)
XLA Modules:
  0.0 29.6 jit_solution(9609654719855895679)
XLA Ops:
  0.6 26.9 %layer.1 = (bf16[16,256]{1,0:T(8,128)(2,1)S(1)}, f32[16,512,128]{2,1,0:T(8,128)S(1)}, bf16[3,16,512]{2,1,0:T(8,128)(2,1)S(1)}) custom-call(bf16[16,2048]{1,0:T(8,128)(2,1)} %tokens_hbm.1, s32[4,16]{1,0:T(4,128)} %bitcast.20, f32[4,16]{1,0:T(4,128)} %bitcast.21, f32[1,2048]{1,0:T(1,128)} %bitcast.17, bf16[2048,512]{1,0:T(8,128)(2,1)} %gate_hbm.1, ...), custom_call_target="tpu_custom_call" | custom-call | tf_op jit(solution)/shard_map/layer/pallas_call | solution.py:605
  27.6 2.0 %finish.1 = (bf16[16,256]{1,0:T(8,128)(2,1)}, f32[16,512,128]{2,1,0:T(8,128)}, bf16[3,16,512]{2,1,0:T(8,128)(2,1)}) custom-call(bf16[16,256]{1,0:T(8,128)(2,1)S(1)} %get-tuple-element.9.out_in, f32[16,512,128]{2,1,0:T(8,128)S(1)} %get-tuple-element.10.new_in, bf16[3,16,512]{2,1,0:T(8,128)(2,1)S(1)} %get-tuple-element.11.filter_in), custom_call_target="tpu_custom_call" | custom-call | tf_op jit(solution)/shard_map/finish/pallas_call | solution.py:643
